TPU v7x, 256 devices: a 2x2x32 block of a 4x8x32 slice. The times are simulated.
256 devices in a mesh: grp: 4 (over y, x), ep: 64 (over z, core).
Axes of the slice: x: 2, y: 2, z: 32, core: 2. Of those that a mesh axis runs over, the one named last changes fastest.
The devices are a block of a 4x8x32 slice.
Arguments:
- tokens: bfloat16 [65536, 2048], P(('grp', 'ep')), parts along dimension 0, may hold values from -6 to 6
- norm_gain: float32 [2048], replicated, may hold values from 0.1 to 1.9
- route_ids: int32 [65536, 2], P(('grp', 'ep')), parts along dimension 0, may hold values from 0 to 63, as said below
- route_slots: int32 [65536, 2], P(('grp', 'ep')), parts along dimension 0, may hold values from 0 to 11, as said below
- route_weights: float32 [65536, 2], P(('grp', 'ep')), parts along dimension 0, may hold values from 0.1 to 1
- w_gate: bfloat16 [64, 2048, 512], P('ep'), may hold values from -0.125 to 0.125
- w_up: bfloat16 [64, 2048, 512], P('ep'), may hold values from -0.125 to 0.125
- w_down: bfloat16 [64, 512, 2048], P('ep'), may hold values from -0.25 to 0.25
Outputs:
- expert_mix: bfloat16 [65536, 2048], P(('grp', 'ep')), parts along dimension 0
There are 4 independent parts, one for each index of `grp`. A program takes and returns all parts, laid end to end along the dimension named above; an argument that names none is the same for every part. Nothing has to cross between parts.
Inputs may be any that keep to these rules, and one draw needn't show every extreme that they name: `route_ids`: expert e belongs to group e // 16. Each token names 2 different experts of one group. In each aligned block of 256 tokens (the rows of one device) no expert is named more than 12 times, and some expert exactly 12 times. `route_slots`: in each aligned block of 256 tokens, the entries that name one expert hold distinct slots 0, 1, ... up to their count less one.
All inputs are finite; a program needn't handle non-finite values.
Results may differ from a plain program's by a relative error of at most 0.007.
Values may be sent and summed in bfloat16 or wider, within the bound.
A program may use at most 64 MiB of HBM per device.

v0:
```python
import jax
import jax.numpy as jnp
from jax import lax
from jax.sharding import Mesh
from jax.sharding import PartitionSpec as P

EP = ("ep_0", "ep_1")
GRP_EP = ("grp", "ep_0", "ep_1")


def cut_along(shard, dim, size):
    before, after = (shard.shape[:dim], shard.shape[dim + 1 :])
    return jnp.moveaxis(shard.reshape(*before, size, -1, *after), dim, 0)


def joined_along(pieces, dim):
    pieces = jnp.moveaxis(pieces, 0, dim)
    dims = pieces.shape
    return pieces.reshape(*dims[:dim], dims[dim] * dims[dim + 1], *dims[dim + 2 :])


def exchange_in_order(pieces, axes, order):
    dims = [lax.axis_size(a) for a in axes]
    pieces = pieces.reshape(*dims, *pieces.shape[1:])
    for k in order:
        pieces = lax.all_to_all(pieces, axes[k], split_axis=k, concat_axis=k, tiled=True)
    return pieces.reshape(-1, *pieces.shape[len(axes) :])


def exchange_by_chip(shard, groups, order, split_dim, concat_dim):
    size = lax.axis_size(groups[0]) * lax.axis_size(groups[1])
    pieces = cut_along(shard, split_dim, size)
    return joined_along(exchange_in_order(pieces, groups, order), concat_dim)


def shards(tokens, norm_gain, route_ids, route_slots, route_weights, w_gate, w_up, w_down):
    tok_rows = tokens.shape[0]
    feat_dim = tokens.shape[1]
    n_devices = lax.axis_size(EP)
    local_count = w_gate.shape[0]
    experts_all = n_devices * local_count
    top_count = route_ids.shape[1]
    capacity = 3 * top_count * tok_rows // (2 * experts_all)
    tok_f32 = tokens.astype(jnp.float32)
    scale = lax.rsqrt(jnp.mean(tok_f32 * tok_f32, axis=-1, keepdims=True) + 1e-06)
    normed = (tok_f32 * scale * norm_gain).astype(jnp.bfloat16)
    place_idx = (route_ids * capacity + route_slots).reshape(-1)
    send = jnp.zeros((experts_all * capacity, feat_dim), jnp.bfloat16)
    send = send.at[place_idx].set(jnp.repeat(normed, top_count, axis=0))
    send = send.reshape(n_devices, local_count, capacity, feat_dim)
    half_cap = capacity // 2
    pieces = []
    for portion in range(2):
        part_send = send[:, :, portion * half_cap : (portion + 1) * half_cap]
        rows_in = lax.all_to_all(part_send, EP, split_axis=0, concat_axis=0, tiled=True)
        gate_act = jnp.einsum("sxcd,xdf->sxcf", rows_in, w_gate, preferred_element_type=jnp.float32)
        up_act = jnp.einsum("sxcd,xdf->sxcf", rows_in, w_up, preferred_element_type=jnp.float32)
        hidden = (jax.nn.silu(gate_act) * up_act).astype(jnp.bfloat16)
        part_done = jnp.einsum(
            "sxcf,xfd->sxcd", hidden, w_down, preferred_element_type=jnp.float32
        ).astype(jnp.bfloat16)
        pieces.append(exchange_by_chip(part_done, ("ep_0", "ep_1"), (0, 1), 0, 0))
    returned = jnp.concatenate(pieces, axis=2)
    flat_rows = returned.reshape(experts_all * capacity, feat_dim)
    picked = flat_rows[place_idx].reshape(tok_rows, top_count, feat_dim).astype(jnp.float32)
    mixed = jnp.sum(route_weights[:, :, None] * picked, axis=1)
    return mixed.astype(jnp.bfloat16)


def solution(mesh):
    torus = Mesh(mesh.devices.reshape(mesh.shape["grp"], 32, 2), ("grp", "ep_0", "ep_1"))
    in_specs = (
        P(GRP_EP, None),
        P(),
        P(GRP_EP, None),
        P(GRP_EP, None),
        P(GRP_EP, None),
        P(EP, None, None),
        P(EP, None, None),
        P(EP, None, None),
    )
    out_specs = P(GRP_EP, None)
    return jax.shard_map(
        shards, mesh=torus, in_specs=in_specs, out_specs=out_specs, check_vma=False
    )
```

profile of v0, /device:TPU:37, one launch (start us, length us, event | category | flops | bytes accessed | tf_op | source)
XLA Modules:
  0.0 834.6 jit_solution(11675043686818631652)
XLA Ops:
  4.2 2.6 broadcast_in_dim.5
  6.8 4.1 reshape.111
  10.9 6.7 scatter_custom_fusion
  17.6 6.1 reshape.89
  23.7 5.2 slice_bitcast_fusion.1
  28.9 231.6 %all_to_all.30 = bf16[64,1,6,2048]{3,2,1,0:T(8,128)(2,1)} all-to-all(bf16[64,1,6,2048]{3,2,1,0:T(8,128)(2,1)S(1)} %get-tuple-element.5), channel_id=1, replica_groups=mesh['grp'=4,'ep_0'=32,'ep_1'=2] {'ep_0','ep_1'}, dimensions={0} | all-to-all | bytes 3145728 | tf_op jit(solution)/shard_map/all_to_all | solution.py:55
  260.5 9.1 %all-to-all-start.3 = ((bf16[64,1,6,2048]{3,2,1,0:T(8,128)(2,1)}), bf16[64,1,6,2048]{3,2,1,0:T(8,128)(2,1)}, u32[]{:S(2)}, u32[]{:S(2)}) async-start(bf16[64,1,6,2048]{3,2,1,0:T(8,128)(2,1)} %get-tuple-element.6), calls=%async_computation.3 | async-start | bytes 4194304 | tf_op jit(solution)/shard_map/all_to_all | solution.py:55
  269.7 3.4 fusion.21
  273.0 5.5 fusion
  278.5 3.8 reshape_reshape.12
  282.3 4.3 copy.32
  286.5 181.0 %all-to-all-done.3 = bf16[64,1,6,2048]{3,2,1,0:T(8,128)(2,1)} async-done(((bf16[64,1,6,2048]{3,2,1,0:T(8,128)(2,1)}), bf16[64,1,6,2048]{3,2,1,0:T(8,128)(2,1)}, u32[]{:S(2)}, u32[]{:S(2)}) %all-to-all-start.3) | async-done | bytes 1572896 | tf_op jit(solution)/shard_map/all_to_all | solution.py:55
  467.5 5.5 all-to-all-start.1
  473.0 3.3 fusion.26
  476.4 5.5 fusion.1
  481.9 2.8 reshape_reshape.14
  484.7 2.9 copy.37
  487.6 133.3 %all-to-all-done.1 = bf16[32,2,1,1,6,2048]{5,1,4,3,2,0:T(2,128)(2,1)} async-done(((bf16[32,2,1,1,6,2048]{5,1,4,3,2,0:T(2,128)(2,1)}), bf16[32,2,1,1,6,2048]{5,1,4,3,2,0:T(2,128)(2,1)}, u32[]{:S(2)}, u32[]{:S(2)}) %all-to-all-start.1) | async-done | bytes 1572896 | tf_op jit(solution)/shard_map/all_to_all | solution.py:26
  620.9 2.3 copy.33
  623.2 12.2 %all_to_all.31 = bf16[32,2,1,1,6,2048]{5,0,4,3,2,1:T(8,128)(2,1)S(1)} all-to-all(bf16[32,2,1,1,6,2048]{5,0,4,3,2,1:T(8,128)(2,1)S(1)} %copy.33), channel_id=1, replica_groups=mesh['grp'=4,'ep_0'=32,'ep_1'=2] {'ep_1'}, dimensions={1} | all-to-all | bytes 3145728 | tf_op jit(solution)/shard_map/all_to_all | solution.py:26
  635.3 5.2 all-to-all-start.4
  640.7 2.8 copy.34
  643.5 2.5 reshape_reshape.13
  646.0 142.0 %all-to-all-done.4 = bf16[32,2,1,1,6,2048]{5,1,4,3,2,0:T(2,128)(2,1)S(1)} async-done(((bf16[32,2,1,1,6,2048]{5,1,4,3,2,0:T(2,128)(2,1)}), bf16[32,2,1,1,6,2048]{5,1,4,3,2,0:T(2,128)(2,1)S(1)}, u32[]{:S(2)}, u32[]{:S(2)}) %all-to-all-start.4) | async-done | bytes 1572896 | tf_op jit(solution)/shard_map/all_to_all | solution.py:26
  788.9 12.5 %all_to_all.32 = bf16[32,2,1,1,6,2048]{5,0,4,3,2,1:T(8,128)(2,1)S(1)} all-to-all(bf16[32,2,1,1,6,2048]{5,0,4,3,2,1:T(8,128)(2,1)S(1)} %copy.38), channel_id=1, replica_groups=mesh['grp'=4,'ep_0'=32,'ep_1'=2] {'ep_1'}, dimensions={1} | all-to-all | bytes 3145728 | tf_op jit(solution)/shard_map/all_to_all | solution.py:26
  803.0 2.0 reshape_reshape.15
  805.0 1.7 pad_maximum_fusion
  806.7 3.7 copy.40
  810.4 4.7 reshape.97
  815.1 3.3 gather_fusion
  818.5 5.8 reshape.98
  824.3 9.9 %multiply_reduce_fusion = bf16[256,2048]{1,0:T(8,128)(2,1)} fusion(f32[256,2,2048]{2,1,0:T(2,128)} %reshape.98, f32[256,2]{1,0:T(8,128)S(1)} %copy.28), kind=kLoop, calls=%fused_computation.2 | loop fusion | flops 1572864 | bytes 5244928 | tf_op jit(solution)/shard_map/reduce_sum | solution.py:66
  (17 shorter events, 6.8 us)
Async XLA Ops:
  0.0 273.0 %copy-start = (bf16[1,512,2048]{2,1,0:T(8,128)(2,1)S(1)}, bf16[1,512,2048]{2,1,0:T(8,128)(2,1)}, u32[]{:S(2)}) copy-start(bf16[1,512,2048]{2,1,0:T(8,128)(2,1)} %param.15) | copy-start | bytes 6291460
  260.5 207.0 %all-to-all-start.3 = ((bf16[64,1,6,2048]{3,2,1,0:T(8,128)(2,1)}), bf16[64,1,6,2048]{3,2,1,0:T(8,128)(2,1)}, u32[]{:S(2)}, u32[]{:S(2)}) async-start(bf16[64,1,6,2048]{3,2,1,0:T(8,128)(2,1)} %get-tuple-element.6), calls=%async_computation.3 | async-start | bytes 4194304 | tf_op jit(solution)/shard_map/all_to_all | solution.py:55
  467.5 153.4 %all-to-all-start.1 = ((bf16[32,2,1,1,6,2048]{5,1,4,3,2,0:T(2,128)(2,1)}), bf16[32,2,1,1,6,2048]{5,1,4,3,2,0:T(2,128)(2,1)}, u32[]{:S(2)}, u32[]{:S(2)}) async-start(bf16[32,2,1,1,6,2048]{5,1,4,3,2,0:T(2,128)(2,1)} %copy.32), calls=%async_computation.1 | async-start | bytes 3145728 | tf_op jit(solution)/shard_map/all_to_all | solution.py:26
  635.3 5.2 copy-start.2
  635.3 152.7 %all-to-all-start.4 = ((bf16[32,2,1,1,6,2048]{5,1,4,3,2,0:T(2,128)(2,1)}), bf16[32,2,1,1,6,2048]{5,1,4,3,2,0:T(2,128)(2,1)S(1)}, u32[]{:S(2)}, u32[]{:S(2)}) async-start(bf16[32,2,1,1,6,2048]{5,1,4,3,2,0:T(2,128)(2,1)} %copy.37), calls=%async_computation.4 | async-start | bytes 3145728 | tf_op jit(solution)/shard_map/all_to_all | solution.py:26
  818.5 15.7 %copy-start.1 = (bf16[1,512,2048]{2,1,0:T(8,128)(2,1)S(1)}, bf16[1,512,2048]{2,1,0:T(8,128)(2,1)}, u32[]{:S(2)}) copy-start(bf16[1,512,2048]{2,1,0:T(8,128)(2,1)} %param.15) | copy-start | bytes 6291460
where the time goes:
time: 844 us; the launch traced here: 835 us
  waiting for transfers between devices  456 us (54%)
  blocking collectives  256 us (30%)
  local copies, waits for them, and re-layouts  68.4 us (8%)
  starting transfers between devices  19.9 us (2%)
  matrix products  17.7 us (2%)
  other arithmetic  15.5 us (2%)
    all_to_all x2, waiting for transfers between devices, exchange_in_order(): lax.all_to_all(pieces, axes[k], split_axis=k, concat_axis=k, tiled=True)  275 us
    all_to_all x1, blocking collectives, shards(): lax.all_to_all(part_send, EP, split_axis=0, concat_axis=0, tiled=True)  232 us
    all_to_all x1, waiting for transfers between devices, shards(): lax.all_to_all(part_send, EP, split_axis=0, concat_axis=0, tiled=True)  181 us
    all_to_all x2, blocking collectives, exchange_in_order(): lax.all_to_all(pieces, axes[k], split_axis=k, concat_axis=k, tiled=True)  24.7 us
  transfers between devices with their start and end apart: 3, of which 3 were waited for; matrix products, arithmetic and copies ran while one was open for 4% of the time, Pallas kernels for 0%

commit v1 on v0

v1 whole, which is shorter than its diff:
```python
import functools

import jax
import jax.numpy as jnp
from jax import lax
from jax.experimental import pallas as pl
from jax.experimental.pallas import tpu as pltpu
from jax.sharding import PartitionSpec as P

MESH = pl.DeviceIdType.MESH
GROUP = 16
HALF = GROUP // 2
CUTS = 4
F32 = jnp.float32
BF16 = jnp.bfloat16


def onehot(mask):
    return jnp.where(mask, 1.0, 0.0).astype(BF16)


def iota(shape, dim):
    return lax.broadcasted_iota(jnp.int32, shape, dim).astype(F32)


def exact_dot_nt(a, b):
    return lax.dot_general(
        a, b, (((1,), (1,)), ((), ())), precision=lax.Precision.HIGHEST, preferred_element_type=F32
    )


def dot(a, b):
    return jnp.dot(a, b, preferred_element_type=F32)


def kernel(
    n, cap, bundle, tab_ref, tok_ref, gain_ref, wg_hbm, wu_hbm, wd_hbm, out_ref,
    wg, wu, wd, nrm, pick, bout, bin_, mout, min_, xs, xin, zs, zin, rs, rin, xstk, ystk, perm, place,
    wsem, bsend, brecv, msend, mrecv, xsend, xrecv, zsend, zrecv, rsend, rrecv,
):
    toks, feats = tok_ref.shape
    piece = feats // CUTS
    unit = CUTS * cap
    rows = GROUP * unit
    quad = 4 * unit
    slots = 4
    me = lax.axis_index("ep")
    base = (me // GROUP) * GROUP
    r = me % GROUP
    upper = (r // HALF)
    sign = 2 * upper - 1

    def wrap(dev):
        return (dev + 4 * n) % n

    def target(k):
        return wrap(me + sign * (2 * (k % 2) - 1) * HALF * k)

    def source(k):
        return wrap(me + sign * HALF * k)

    copies = [
        pltpu.make_async_copy(src, dst, wsem.at[i])
        for i, (src, dst) in enumerate(((wg_hbm.at[0], wg), (wu_hbm.at[0], wu), (wd_hbm.at[0], wd)))
    ]
    for c in copies:
        c.start()

    barrier = pltpu.get_barrier_semaphore()

    def greet(i, _):
        pl.semaphore_signal(barrier, inc=1, device_id={"ep": base + (r + i) % GROUP}, device_id_type=MESH)
        return 0

    bin_[:, :, bundle:, :] = jnp.zeros_like(bin_[:, :, bundle:, :])
    for k in range(slots):
        lo = k * 128 + bundle
        rin[:, lo : lo + 128 - bundle, :] = jnp.zeros((CUTS, 128 - bundle, piece), BF16)

    lax.fori_loop(1, GROUP, greet, 0)
    for other in (wrap(me + HALF * sign), wrap(me + 3 * HALF * sign), wrap(me + 2 * HALF), wrap(me - 2 * HALF)):
        pl.semaphore_signal(barrier, inc=1, device_id={"ep": other}, device_id_type=MESH)

    step = 32
    gain = gain_ref[...]

    def norm(i, _):
        at = pl.ds(pl.multiple_of(i * step, step), step)
        x = tok_ref[at, :].astype(F32)
        scale = lax.rsqrt(jnp.mean(x * x, axis=-1, keepdims=True) + 1e-06)
        nrm[at, :] = (x * scale * gain).astype(BF16)
        return 0

    lax.fori_loop(0, toks // step, norm, 0)

    tab = tab_ref[...]
    slot_row = tab[0:1, :]
    of_slot = onehot(iota((8, toks), 0) == slot_row)
    before = onehot(iota((toks, toks), 0) < iota((toks, toks), 1))
    ranks = dot(of_slot, before)
    rank_row = jnp.sum(of_slot.astype(F32) * ranks, axis=0, keepdims=True)
    key_row = slot_row * 128.0 + rank_row
    mask = iota((slots * 128, toks), 0) == key_row
    pick[...] = onehot(mask)
    meta = exact_dot_nt(tab, jnp.where(mask, 1.0, 0.0).astype(F32))
    for k in range(slots):
        mout[k] = meta[:, k * 128 : (k + 1) * 128]
    eye = jnp.where(iota((toks, toks), 0) == iota((toks, toks), 1), 1.0, 0.0).astype(F32)
    key_col = exact_dot_nt(eye, jnp.broadcast_to(key_row, (8, toks)))[:, 0:1]
    place[...] = onehot(iota((toks, slots * 128), 1) == key_col)

    for c in range(CUTS):
        bout[c] = dot(pick[...], nrm[:, c * piece : (c + 1) * piece]).astype(BF16)

    i0 = iota((quad, quad), 0)
    a0 = jnp.floor((i0 + 0.5) / unit)
    b0 = jnp.floor((i0 - a0 * unit + 0.5) / cap)
    swapped = b0 * unit + a0 * cap + (i0 - a0 * unit - b0 * cap)
    perm[...] = onehot(iota((quad, quad), 1) == swapped)

    pl.semaphore_wait(barrier, GROUP - 1 + 4)

    def send_bundle(k):
        pltpu.make_async_remote_copy(
            src_ref=mout.at[k], dst_ref=min_.at[k], send_sem=msend.at[k], recv_sem=mrecv.at[k],
            device_id={"ep": target(k)}, device_id_type=MESH,
        ).start()
        pltpu.make_async_remote_copy(
            src_ref=bout.at[:, pl.ds(k * 128, bundle)], dst_ref=bin_.at[k, :, pl.ds(0, bundle)],
            send_sem=bsend.at[k], recv_sem=brecv.at[k],
            device_id={"ep": target(k)}, device_id_type=MESH,
        ).start()

    own_meta = pltpu.make_async_copy(mout.at[0], min_.at[0], mrecv.at[0])
    own_rows = pltpu.make_async_copy(bout.at[:, pl.ds(0, bundle)], bin_.at[0, :, pl.ds(0, bundle)], brecv.at[0])
    own_meta.start()
    own_rows.start()
    for k in range(1, slots):
        send_bundle(k)

    def spread(src, dst, k, send_sem, recv_sem):
        mine = pl.ds(pl.multiple_of(r * unit, 16), unit)

        def one(i, _):
            other = (r + i) % GROUP
            pltpu.make_async_remote_copy(
                src_ref=src.at[k, pl.ds(pl.multiple_of(other * unit, 16), unit)], dst_ref=dst.at[k, mine],
                send_sem=send_sem.at[k], recv_sem=recv_sem.at[k],
                device_id={"ep": base + other}, device_id_type=MESH,
            ).start()
            return 0

        lax.fori_loop(1, GROUP, one, 0)
        pltpu.make_async_copy(src.at[k, mine], dst.at[k, mine], recv_sem.at[k]).start()

    def landed(ref, sem):
        pltpu.make_async_copy(ref, ref, sem).wait()

    def gather(k):
        landed(min_.at[k], mrecv.at[k])
        landed(bin_.at[k, :, pl.ds(0, bundle)], brecv.at[k])
        m = min_[k]
        both = []
        for i in (1, 2):
            j = jnp.where(m[i : i + 1] > 0.0, m[i : i + 1] - 1.0, -1000.0)
            both.append(jnp.concatenate([j + float(cap * c) for c in range(CUTS)], axis=1))

        def part(b, _):
            at = pl.ds(pl.multiple_of(b * quad, quad), quad)
            row = iota((quad, CUTS * 128), 0) + (b * quad).astype(F32)
            sel = onehot((row == both[0]) | (row == both[1]))
            xs[k, at, :] = dot(sel, bin_[k].reshape(CUTS * 128, piece)).astype(BF16)
            return 0

        lax.fori_loop(0, 4, part, 0)
        spread(xs, xin, k, xsend, xrecv)

    def expert(k):
        landed(xin.at[k], xrecv.at[k])
        for b in range(4):
            y = dot(perm[...], xin[k, b * quad : (b + 1) * quad, :]).astype(BF16)
            for c in range(CUTS):
                xstk[b * unit : (b + 1) * unit, c * piece : (c + 1) * piece] = y[c * unit : (c + 1) * unit]
        gate = dot(xstk[...], wg[...])
        up = dot(xstk[...], wu[...])
        hidden = (gate / (1.0 + jnp.exp(-gate)) * up).astype(BF16)
        for c in range(CUTS):
            y = dot(hidden, wd[:, c * piece : (c + 1) * piece]).astype(BF16)
            for b in range(4):
                ystk[b, c * unit : (c + 1) * unit, :] = y[b * unit : (b + 1) * unit]
        for b in range(4):
            zs[k, b * quad : (b + 1) * quad, :] = dot(perm[...], ystk[b]).astype(BF16)
        spread(zs, zin, k, zsend, zrecv)

    def combine(k):
        landed(zin.at[k], zrecv.at[k])
        eye = jnp.where(iota((128, 128), 0) == iota((128, 128), 1), 1.0, 0.0).astype(F32)
        cols = exact_dot_nt(eye, min_[k])
        j1 = jnp.where(cols[:, 1:2] > 0.0, cols[:, 1:2] - 1.0, -1000.0)
        j2 = jnp.where(cols[:, 2:3] > 0.0, cols[:, 2:3] - 1.0, -1000.0)
        w1, w2 = cols[:, 3:4], cols[:, 4:5]
        lane = iota((128, rows), 1)
        for c in range(CUTS):
            y1 = dot(onehot(lane == j1 + float(cap * c)), zin[k])
            y2 = dot(onehot(lane == j2 + float(cap * c)), zin[k])
            rs[k, c] = (w1 * y1 + w2 * y2).astype(BF16)
        dst = rin.at[:, pl.ds(pl.multiple_of(k * 128, 128), bundle)]

        @pl.when(k == 0)
        def _():
            pltpu.make_async_copy(rs.at[0, :, pl.ds(0, bundle)], dst, rrecv.at[0]).start()

        @pl.when(k > 0)
        def _():
            pltpu.make_async_remote_copy(
                src_ref=rs.at[k, :, pl.ds(0, bundle)], dst_ref=dst, send_sem=rsend.at[k], recv_sem=rrecv.at[k],
                device_id={"ep": source(k)}, device_id_type=MESH,
            ).start()

    def stage(t, _):
        @pl.when(t < slots)
        def _():
            gather(t)

        @pl.when(t == 1)
        def _():
            for c in copies:
                c.wait()

        @pl.when((t >= 1) & (t < slots + 1))
        def _():
            expert(t - 1)

        @pl.when(t >= 2)
        def _():
            combine(t - 2)

        return 0

    lax.fori_loop(0, slots + 2, stage, 0)

    for k in range(slots):
        landed(rin.at[:, pl.ds(k * 128, bundle)], rrecv.at[k])
    for c in range(CUTS):
        out_ref[:, c * piece : (c + 1) * piece] = dot(place[...], rin[c]).astype(BF16)

    for k in range(slots):
        for buf, sem in ((xs, xsend), (zs, zsend)):
            landed(buf.at[k, pl.ds(0, rows - unit)], sem.at[k])
    for k in range(1, slots):
        landed(mout.at[k], msend.at[k])
        landed(bout.at[:, pl.ds(k * 128, bundle)], bsend.at[k])
        landed(rs.at[k, :, pl.ds(0, bundle)], rsend.at[k])


def shards(n, tokens, norm_gain, route_ids, route_slots, route_weights, w_gate, w_up, w_down):
    toks, feats = tokens.shape
    hidden = w_gate.shape[2]
    top = route_ids.shape[1]
    cap = 3 * top * toks // (2 * n)
    bundle = GROUP * cap // top
    piece = feats // CUTS
    unit = CUTS * cap
    rows = GROUP * unit
    slots = 4

    me = lax.axis_index("ep")
    rel = (route_ids[:, 0] // GROUP - me // GROUP + slots) % slots
    lower = (me % GROUP) < HALF
    first = jnp.where(lower, 3, 1)
    slot = jnp.where(rel == 0, 0, jnp.where(rel == 2, 3, jnp.where(rel == first, 1, 2)))
    spots = (route_ids % GROUP) * unit + route_slots + 1
    zero = jnp.zeros((toks,), F32)
    tab = jnp.stack(
        [slot.astype(F32), spots[:, 0].astype(F32), spots[:, 1].astype(F32), route_weights[:, 0], route_weights[:, 1],
         zero, zero, zero]
    )
    vmem = pl.BlockSpec(memory_space=pltpu.VMEM)
    hbm = pl.BlockSpec(memory_space=pl.ANY)
    return pl.pallas_call(
        functools.partial(kernel, n, cap, bundle),
        out_shape=jax.ShapeDtypeStruct((toks, feats), BF16),
        in_specs=[vmem, vmem, vmem, hbm, hbm, hbm],
        out_specs=vmem,
        scratch_shapes=[
            pltpu.VMEM((feats, hidden), BF16),
            pltpu.VMEM((feats, hidden), BF16),
            pltpu.VMEM((hidden, feats), BF16),
            pltpu.VMEM((toks, feats), BF16),
            pltpu.VMEM((slots * 128, toks), BF16),
            pltpu.VMEM((CUTS, slots * 128, piece), BF16),
            pltpu.VMEM((slots, CUTS, 128, piece), BF16),
            pltpu.VMEM((slots, 8, 128), F32),
            pltpu.VMEM((slots, 8, 128), F32),
            pltpu.VMEM((slots, rows, piece), BF16),
            pltpu.VMEM((slots, rows, piece), BF16),
            pltpu.VMEM((slots, rows, piece), BF16),
            pltpu.VMEM((slots, rows, piece), BF16),
            pltpu.VMEM((slots, CUTS, 128, piece), BF16),
            pltpu.VMEM((CUTS, slots * 128, piece), BF16),
            pltpu.VMEM((GROUP * cap, feats), BF16),
            pltpu.VMEM((4, 4 * unit, piece), BF16),
            pltpu.VMEM((4 * unit, 4 * unit), BF16),
            pltpu.VMEM((toks, slots * 128), BF16),
            pltpu.SemaphoreType.DMA((3,)),
        ] + [pltpu.SemaphoreType.DMA((slots,))] * 10,
        compiler_params=pltpu.CompilerParams(
            collective_id=0, has_side_effects=True, vmem_limit_bytes=60 * 1024 * 1024
        ),
    )(tab, tokens, norm_gain.reshape(1, feats), w_gate, w_up, w_down)


def solution(mesh):
    both = ("grp", "ep")
    in_specs = (
        P(both, None), P(None), P(both, None), P(both, None), P(both, None),
        P("ep", None, None), P("ep", None, None), P("ep", None, None),
    )
    return jax.shard_map(
        functools.partial(shards, mesh.shape["ep"]), mesh=mesh, in_specs=in_specs, out_specs=P(both, None),
        check_vma=False,
    )
```

time: 844 us -> 492 us (0.58)
  the two profiles are of different devices: /device:TPU:37 before, /device:TPU:751 now
where the time goes in v1:
time: 492 us
  Pallas kernels  487 us (99%)
    pallas_call x1, Pallas kernels, shards(): pl.pallas_call(functools.partial(kernel, n, cap, bundle), out_shape=jax.S...  487 us

profile of v1, /device:TPU:751, one launch (start us, length us, event | category | flops | bytes accessed | tf_op | source)
XLA Modules:
  0.0 491.6 jit_solution(8782692199323429750)
XLA Ops:
  0.0 0.7 fusion.4
  0.7 0.7 fusion.3
  1.4 0.8 slice_bitcast_fusion
  2.2 0.6 stack.10.tab_ref
  2.8 486.5 %shard_map.82 = bf16[256,2048]{1,0:T(8,128)(2,1)} custom-call(f32[8,256]{1,0:T(8,128)} %stack.10.tab_ref, bf16[256,2048]{1,0:T(8,128)(2,1)} %tok_ref.1, f32[1,2048]{1,0:T(1,128)} %bitcast.19, bf16[1,2048,512]{2,1,0:T(8,128)(2,1)} %wg_hbm.1, bf16[1,2048,512]{2,1,0:T(8,128)(2,1)} %wu_hbm.1, bf16[1,512,2048]{2,1,0:T(8,128)(2,1)} %wd_hbm.1), custom_call_target="tpu_custom_call" | custom-call | tf_op jit(solution)/shard_map/pallas_call | solution.py:280
  489.3 2.3 copy.10
  (3 shorter events, 0.0 us)

commit v2 on v1

--- a/solution.py
+++ b/solution.py
@@ -11,8 +11,16 @@
 GROUP = 16
 HALF = GROUP // 2
 CUTS = 4
+SENDS = (3, 2, 1)
+ET, CT = 2, 3
+
 F32 = jnp.float32
 BF16 = jnp.bfloat16
+
+
+def far_order(one, r):
+    lax.fori_loop(0, GROUP - 1 - r, lambda i, a: one(GROUP - 1 - i, a), 0)
+    lax.fori_loop(0, r, one, 0)
 
 
 def onehot(mask):
@@ -34,11 +42,11 @@
 
 
 def kernel(
-    n, cap, bundle, tab_ref, tok_ref, gain_ref, wg_hbm, wu_hbm, wd_hbm, out_ref,
-    wg, wu, wd, nrm, pick, bout, bin_, mout, min_, xs, xin, zs, zin, rs, rin, xstk, ystk, perm, place,
-    wsem, bsend, brecv, msend, mrecv, xsend, xrecv, zsend, zrecv, rsend, rrecv,
+    n, cap, bundle, ids_ref, spots_ref, mix_ref, tok_hbm, gain_ref, wg_hbm, wu_hbm, wd_hbm, out_ref,
+    tok_ref, wg, wu, wd, nrm, pick, bout, bin_, mout, min_, xs, xin, zs, zin, rs, rin, xstk, ystk, perm, place,
+    tsem, wsem, bsend, brecv, msend, mrecv, xsend, xrecv, zsend, zrecv, rsend, rrecv,
 ):
-    toks, feats = tok_ref.shape
+    toks, feats = tok_hbm.shape
     piece = feats // CUTS
     unit = CUTS * cap
     rows = GROUP * unit
@@ -59,6 +67,18 @@
     def source(k):
         return wrap(me + sign * HALF * k)
 
+    barrier = pltpu.get_barrier_semaphore()
+
+    def greet(i, _):
+        pl.semaphore_signal(barrier, inc=1, device_id={"ep": base + (r + i) % GROUP}, device_id_type=MESH)
+        return 0
+
+    lax.fori_loop(1, GROUP, greet, 0)
+    for other in (wrap(me + HALF * sign), wrap(me + 3 * HALF * sign), wrap(me + 2 * HALF), wrap(me - 2 * HALF)):
+        pl.semaphore_signal(barrier, inc=1, device_id={"ep": other}, device_id_type=MESH)
+
+    tokens_in = pltpu.make_async_copy(tok_hbm, tok_ref, tsem)
+    tokens_in.start()
     copies = [
         pltpu.make_async_copy(src, dst, wsem.at[i])
         for i, (src, dst) in enumerate(((wg_hbm.at[0], wg), (wu_hbm.at[0], wu), (wd_hbm.at[0], wd)))
@@ -66,20 +86,10 @@
     for c in copies:
         c.start()
 
-    barrier = pltpu.get_barrier_semaphore()
-
-    def greet(i, _):
-        pl.semaphore_signal(barrier, inc=1, device_id={"ep": base + (r + i) % GROUP}, device_id_type=MESH)
-        return 0
-
     bin_[:, :, bundle:, :] = jnp.zeros_like(bin_[:, :, bundle:, :])
     for k in range(slots):
         lo = k * 128 + bundle
         rin[:, lo : lo + 128 - bundle, :] = jnp.zeros((CUTS, 128 - bundle, piece), BF16)
-
-    lax.fori_loop(1, GROUP, greet, 0)
-    for other in (wrap(me + HALF * sign), wrap(me + 3 * HALF * sign), wrap(me + 2 * HALF), wrap(me - 2 * HALF)):
-        pl.semaphore_signal(barrier, inc=1, device_id={"ep": other}, device_id_type=MESH)
 
     step = 32
     gain = gain_ref[...]
@@ -91,10 +101,16 @@
         nrm[at, :] = (x * scale * gain).astype(BF16)
         return 0
 
+    tokens_in.wait()
     lax.fori_loop(0, toks // step, norm, 0)
 
-    tab = tab_ref[...]
-    slot_row = tab[0:1, :]
+    ids = ids_ref[...]
+    team = ids // GROUP
+    rel = (team[0:1, :] - me // GROUP + slots) % slots
+    near = 3 - 2 * upper
+    slot_row = jnp.where(rel == 0, 0, jnp.where(rel == 2, 3, jnp.where(rel == near, 1, 2))).astype(F32)
+    spots = ((ids - team * GROUP) * unit + spots_ref[...] + 1).astype(F32)
+    tab = jnp.concatenate([slot_row, spots, mix_ref[...], jnp.zeros((3, toks), F32)], axis=0)
     of_slot = onehot(iota((8, toks), 0) == slot_row)
     before = onehot(iota((toks, toks), 0) < iota((toks, toks), 1))
     ranks = dot(of_slot, before)
@@ -135,14 +151,14 @@
     own_rows = pltpu.make_async_copy(bout.at[:, pl.ds(0, bundle)], bin_.at[0, :, pl.ds(0, bundle)], brecv.at[0])
     own_meta.start()
     own_rows.start()
-    for k in range(1, slots):
+    for k in SENDS:
         send_bundle(k)
 
     def spread(src, dst, k, send_sem, recv_sem):
         mine = pl.ds(pl.multiple_of(r * unit, 16), unit)
 
         def one(i, _):
-            other = (r + i) % GROUP
+            other = i
             pltpu.make_async_remote_copy(
                 src_ref=src.at[k, pl.ds(pl.multiple_of(other * unit, 16), unit)], dst_ref=dst.at[k, mine],
                 send_sem=send_sem.at[k], recv_sem=recv_sem.at[k],
@@ -150,7 +166,7 @@
             ).start()
             return 0
 
-        lax.fori_loop(1, GROUP, one, 0)
+        far_order(one, r)
         pltpu.make_async_copy(src.at[k, mine], dst.at[k, mine], recv_sem.at[k]).start()
 
     def landed(ref, sem):
@@ -218,26 +234,26 @@
             ).start()
 
     def stage(t, _):
-        @pl.when(t < slots)
-        def _():
-            gather(t)
+        @pl.when(t < 4)
+        def _():
+            gather((slots - t) % slots)
 
         @pl.when(t == 1)
         def _():
             for c in copies:
                 c.wait()
 
-        @pl.when((t >= 1) & (t < slots + 1))
-        def _():
-            expert(t - 1)
-
-        @pl.when(t >= 2)
-        def _():
-            combine(t - 2)
+        @pl.when((t >= ET) & (t < ET + slots))
+        def _():
+            expert(ET + slots - 1 - t)
+
+        @pl.when((t >= CT) & (t < CT + slots))
+        def _():
+            combine(CT + slots - 1 - t)
 
         return 0
 
-    lax.fori_loop(0, slots + 2, stage, 0)
+    lax.fori_loop(0, CT + slots, stage, 0)
 
     for k in range(slots):
         landed(rin.at[:, pl.ds(k * 128, bundle)], rrecv.at[k])
@@ -264,25 +280,15 @@
     rows = GROUP * unit
     slots = 4
 
-    me = lax.axis_index("ep")
-    rel = (route_ids[:, 0] // GROUP - me // GROUP + slots) % slots
-    lower = (me % GROUP) < HALF
-    first = jnp.where(lower, 3, 1)
-    slot = jnp.where(rel == 0, 0, jnp.where(rel == 2, 3, jnp.where(rel == first, 1, 2)))
-    spots = (route_ids % GROUP) * unit + route_slots + 1
-    zero = jnp.zeros((toks,), F32)
-    tab = jnp.stack(
-        [slot.astype(F32), spots[:, 0].astype(F32), spots[:, 1].astype(F32), route_weights[:, 0], route_weights[:, 1],
-         zero, zero, zero]
-    )
     vmem = pl.BlockSpec(memory_space=pltpu.VMEM)
     hbm = pl.BlockSpec(memory_space=pl.ANY)
     return pl.pallas_call(
         functools.partial(kernel, n, cap, bundle),
         out_shape=jax.ShapeDtypeStruct((toks, feats), BF16),
-        in_specs=[vmem, vmem, vmem, hbm, hbm, hbm],
+        in_specs=[vmem, vmem, vmem, hbm, vmem, hbm, hbm, hbm],
         out_specs=vmem,
         scratch_shapes=[
+            pltpu.VMEM((toks, feats), BF16),
             pltpu.VMEM((feats, hidden), BF16),
             pltpu.VMEM((feats, hidden), BF16),
             pltpu.VMEM((hidden, feats), BF16),
@@ -302,12 +308,13 @@
             pltpu.VMEM((4, 4 * unit, piece), BF16),
             pltpu.VMEM((4 * unit, 4 * unit), BF16),
             pltpu.VMEM((toks, slots * 128), BF16),
+            pltpu.SemaphoreType.DMA,
             pltpu.SemaphoreType.DMA((3,)),
         ] + [pltpu.SemaphoreType.DMA((slots,))] * 10,
         compiler_params=pltpu.CompilerParams(
             collective_id=0, has_side_effects=True, vmem_limit_bytes=60 * 1024 * 1024
         ),
-    )(tab, tokens, norm_gain.reshape(1, feats), w_gate, w_up, w_down)
+    )(route_ids.T, route_slots.T, route_weights.T, tokens, norm_gain.reshape(1, feats), w_gate, w_up, w_down)
 
 
 def solution(mesh):

time: 492 us -> 470 us (0.955)
  the two profiles are of different devices: /device:TPU:751 before, /device:TPU:37 now
where the time goes in v2:
time: 470 us; the launch traced here: 464 us
  Pallas kernels  462 us (98%)
    pallas_call x1, Pallas kernels, shards(): pl.pallas_call(functools.partial(kernel, n, cap, bundle), out_shape=jax.S...  462 us

profile of v2, /device:TPU:37, one launch (start us, length us, event | category | flops | bytes accessed | tf_op | source)
XLA Modules:
  0.0 464.3 jit_solution(15760951065069021716)
XLA Ops:
  0.0 461.9 %shard_map.82 = bf16[256,2048]{1,0:T(8,128)(2,1)} custom-call(s32[2,256]{1,0:T(2,128)} %bitcast.5, s32[2,256]{1,0:T(2,128)} %bitcast.6, f32[2,256]{1,0:T(2,128)} %bitcast.7, bf16[256,2048]{1,0:T(8,128)(2,1)} %tok_hbm.1, f32[1,2048]{1,0:T(1,128)} %bitcast.4, bf16[1,2048,512]{2,1,0:T(8,128)(2,1)} %wg_hbm.1, bf16[1,2048,512]{2,1,0:T(8,128)(2,1)} %wu_hbm.1, ...), custom_call_target="tpu_custom_call" | custom-call | tf_op jit(solution)/shard_map/pallas_call | solution.py:285
  461.9 2.3 copy.10

commit v3 on v2

--- a/solution.py
+++ b/solution.py
@@ -12,15 +12,25 @@
 HALF = GROUP // 2
 CUTS = 4
 SENDS = (3, 2, 1)
-ET, CT = 2, 3
+ET, CT = 2, 4
 
 F32 = jnp.float32
 BF16 = jnp.bfloat16
 
 
 def far_order(one, r):
-    lax.fori_loop(0, GROUP - 1 - r, lambda i, a: one(GROUP - 1 - i, a), 0)
-    lax.fori_loop(0, r, one, 0)
+    def pair(i, _):
+        @pl.when(GROUP - 1 - i > r)
+        def _():
+            one(GROUP - 1 - i, 0)
+
+        @pl.when(i < r)
+        def _():
+            one(i, 0)
+
+        return 0
+
+    lax.fori_loop(0, GROUP, pair, 0)
 
 
 def onehot(mask):

time: 470 us -> 467 us (level)
  no operation moved by 1% of the time
where the time goes in v3:
time: 467 us; the launch traced here: 463 us
  Pallas kernels  460 us (99%)
    pallas_call x1, Pallas kernels, shards(): pl.pallas_call(functools.partial(kernel, n, cap, bundle), out_shape=jax.S...  460 us

profile of v3, /device:TPU:37, one launch (start us, length us, event | category | flops | bytes accessed | tf_op | source)
XLA Modules:
  0.0 462.8 jit_solution(7161465614267398633)
XLA Ops:
  0.0 460.5 %shard_map.82 = bf16[256,2048]{1,0:T(8,128)(2,1)} custom-call(s32[2,256]{1,0:T(2,128)} %bitcast.5, s32[2,256]{1,0:T(2,128)} %bitcast.6, f32[2,256]{1,0:T(2,128)} %bitcast.7, bf16[256,2048]{1,0:T(8,128)(2,1)} %tok_hbm.1, f32[1,2048]{1,0:T(1,128)} %bitcast.4, bf16[1,2048,512]{2,1,0:T(8,128)(2,1)} %wg_hbm.1, bf16[1,2048,512]{2,1,0:T(8,128)(2,1)} %wu_hbm.1, ...), custom_call_target="tpu_custom_call" | custom-call | tf_op jit(solution)/shard_map/pallas_call | solution.py:295
  460.5 2.3 copy.10

commit v4 on v3

--- a/solution.py
+++ b/solution.py
@@ -12,7 +12,7 @@
 HALF = GROUP // 2
 CUTS = 4
 SENDS = (3, 2, 1)
-ET, CT = 2, 4
+ET, CT = 2, 5
 
 F32 = jnp.float32
 BF16 = jnp.bfloat16

time: 467 us -> 474 us (1.015)
  the two profiles are of different devices: /device:TPU:37 before, /device:TPU:293 now
where the time goes in v4:
time: 474 us; the launch traced here: 473 us
  Pallas kernels  471 us (99%)
    pallas_call x1, Pallas kernels, shards(): pl.pallas_call(functools.partial(kernel, n, cap, bundle), out_shape=jax.S...  471 us

profile of v4, /device:TPU:293, one launch (start us, length us, event | category | flops | bytes accessed | tf_op | source)
XLA Modules:
  0.0 473.3 jit_solution(14958137715548545604)
XLA Ops:
  0.0 471.0 %shard_map.82 = bf16[256,2048]{1,0:T(8,128)(2,1)} custom-call(s32[2,256]{1,0:T(2,128)} %bitcast.5, s32[2,256]{1,0:T(2,128)} %bitcast.6, f32[2,256]{1,0:T(2,128)} %bitcast.7, bf16[256,2048]{1,0:T(8,128)(2,1)} %tok_hbm.1, f32[1,2048]{1,0:T(1,128)} %bitcast.4, bf16[1,2048,512]{2,1,0:T(8,128)(2,1)} %wg_hbm.1, bf16[1,2048,512]{2,1,0:T(8,128)(2,1)} %wu_hbm.1, ...), custom_call_target="tpu_custom_call" | custom-call | tf_op jit(solution)/shard_map/pallas_call | solution.py:295
  471.0 2.3 copy.10
